TPU v7x, 256 devices: a whole 4x4x8 slice. The times are simulated.
256 devices in a mesh: ra: 32 (over z, y), cb: 8 (over x, core).
Axes of the slice: x: 4, y: 4, z: 8, core: 2. Of those that a mesh axis runs over, the one named last changes fastest.
Arguments:
- tokens: bfloat16 [128, 2048], P(None, 'ra'), may hold values from -6 to 6
- pre_gain: float32 [2, 2048], P(None, 'ra'), may hold values from 0.1 to 1.9
- post_gain: float32 [2, 2048], P(None, 'ra'), may hold values from 0.1 to 1.9
- gate_weight: bfloat16 [2, 2048, 5632], P(None, 'ra', 'cb'), may hold values from -0.125 to 0.125
- up_weight: bfloat16 [2, 2048, 5632], P(None, 'ra', 'cb'), may hold values from -0.125 to 0.125
- down_weight: bfloat16 [2, 5632, 2048], P(None, 'cb', 'ra'), may hold values from -0.078125 to 0.078125
Outputs:
- mixed: bfloat16 [128, 2048], P(None, 'ra')
All inputs are finite; a program needn't handle non-finite values.
Results may differ from a plain program's by a relative error of at most 0.008.
Values may be sent and summed in bfloat16 or wider, within the bound.
A program may use at most 64 MiB of HBM per device.

v0:
```python
import functools

import jax
import jax.numpy as jnp
from jax import lax
from jax.sharding import Mesh
from jax.sharding import PartitionSpec as P

D = 2048
RA = ("ra_0", "ra_1")


epsilon = 1e-06
residual_scale = 0.25


def sum_by_axis(array, axes, dim):
    for axis in axes:
        array = lax.psum_scatter(array, axis, scatter_dimension=dim, tiled=True)
    return array


def laid_out(tiles, dim):
    tiles = jnp.moveaxis(tiles, 0, dim)
    shape = tiles.shape
    return tiles.reshape(*shape[:dim], shape[dim] * shape[dim + 1], *shape[dim + 2 :])


def gather_in_order(array, axes, order):
    tiles = array
    for k in order:
        tiles = lax.all_gather(tiles, axes[k])
    done = order[::-1]
    back = [done.index(k) for k in range(len(axes))]
    tiles = tiles.transpose(*back, *range(len(axes), tiles.ndim))
    return tiles.reshape(-1, *array.shape)


def gathered_by_axis(array, axes, order, dim):
    return laid_out(gather_in_order(array, axes, order), dim)


def gathered_total(array, axis):
    return lax.all_gather(array, axis).sum(0)


def by_axis(array, axes):
    return functools.reduce(lax.psum, axes, array)


def project(normed, gate_block, up_block, down_block):
    gate_part = jnp.dot(normed, gate_block, preferred_element_type=jnp.float32)
    up_part = jnp.dot(normed, up_block, preferred_element_type=jnp.float32)
    gate_sum, up_sum = (sum_by_axis(gate_part, RA, 1), sum_by_axis(up_part, RA, 1))
    sliced = (jax.nn.silu(gate_sum) * up_sum).astype(jnp.bfloat16)
    hidden = gathered_by_axis(sliced, RA, (0, 1), 1)
    partial_out = jnp.dot(hidden, down_block, preferred_element_type=jnp.float32)
    return gathered_total(partial_out, "cb")


def per_device(tokens, pre_gain, post_gain, gate_weight, up_weight, down_weight):
    stream = tokens.astype(jnp.float32)
    squares = jnp.zeros((stream.shape[0],), jnp.float32)
    squares = by_axis(jnp.sum(stream * stream, axis=1), RA)
    for sublayer in range(pre_gain.shape[0]):
        scale_in = lax.rsqrt(squares / D + epsilon)
        normed = (stream * scale_in[:, None] * pre_gain[sublayer]).astype(jnp.bfloat16)
        branch = project(normed, gate_weight[sublayer], up_weight[sublayer], down_weight[sublayer])
        gained = branch * post_gain[sublayer]
        branch_sq, gained_sq, cross_sum = (
            by_axis(jnp.sum(branch * branch, axis=1), RA),
            by_axis(jnp.sum(gained * gained, axis=1), RA),
            by_axis(jnp.sum(stream * gained, axis=1), RA),
        )
        scale_out = lax.rsqrt(branch_sq / D + epsilon)
        squares = (
            residual_scale * residual_scale * squares
            + 2.0 * residual_scale * scale_out * cross_sum
            + scale_out * scale_out * gained_sq
        )
        stream = residual_scale * stream + gained * scale_out[:, None]
    return stream.astype(jnp.bfloat16)


def solution(mesh):
    split = Mesh(mesh.devices.reshape(8, 4, mesh.shape["cb"]), ("ra_0", "ra_1", "cb"))
    return jax.shard_map(
        per_device,
        mesh=split,
        in_specs=(
            P(None, RA),
            P(None, RA),
            P(None, RA),
            P(None, RA, "cb"),
            P(None, RA, "cb"),
            P(None, "cb", RA),
        ),
        out_specs=P(None, RA),
        check_vma=False,
    )
```

profile of v0, /device:TPU:1, one launch (start us, length us, event | category | flops | bytes accessed | tf_op | source)
XLA Modules:
  0.0 379.1 jit_solution(12317527957275074624)
XLA Ops:
  6.5 0.8 fusion.23
  7.3 17.3 %psum.70 = f32[128]{0:T(128)S(1)} all-reduce(f32[128]{0:T(128)S(1)} %fusion.23), channel_id=1, replica_groups=mesh['ra_0'=8,'ra_1'=4,'cb'=8] {'ra_0'}, use_global_device_ids=true, to_apply=%region_1.0 | all-reduce | flops 128 | bytes 1024 | tf_op jit(solution)/shard_map/psum | solution.py:48
  24.6 8.7 %psum.71 = f32[128]{0:T(128)S(1)} all-reduce(f32[128]{0:T(128)S(1)} %psum.70), channel_id=1, replica_groups=mesh['ra_0'=8,'ra_1'=4,'cb'=8] {'ra_1'}, use_global_device_ids=true, to_apply=%region_2.0 | all-reduce | flops 128 | bytes 1024 | tf_op jit(solution)/shard_map/psum | solution.py:48
  33.4 0.7 copy-done.4
  34.0 1.9 fusion.12
  36.0 0.9 copy-done.3
  36.9 1.0 fusion.14
  38.0 31.5 %reduce-scatter.23.cloned.1.call-done = f32[128,88]{0,1:T(8,128)} async-done(((f32[128,704]{0,1:T(8,128)}), f32[128,88]{0,1:T(8,128)}) %reduce-scatter.23.cloned.1.call-update) | async-done | bytes 45072
  69.5 38.7 %reduce-scatter.21.cloned.1.call-done = f32[128,88]{0,1:T(8,128)} async-done(((f32[128,704]{0,1:T(8,128)}), f32[128,88]{0,1:T(8,128)}) %reduce-scatter.21.cloned.1.call-update) | async-done | bytes 45072
  108.1 10.2 %fusion.32 = (f32[128,32]{0,1:T(8,128)S(1)}, f32[128,32]{0,1:T(8,128)S(1)}) fusion(f32[128,88]{0,1:T(8,128)} %reduce-scatter.23.cloned.1.call-done, f32[128,88]{0,1:T(8,128)} %reduce-scatter.21.cloned.1.call-done), kind=kCustom, calls=%all-reduce-scatter.5 | all-reduce-scatter fusion | flops 32769 | bytes 123904
  118.4 1.3 collective-permute-start
  119.7 2.8 collective-permute-start.1
  122.5 0.7 copy-done.6
  124.8 18.2 %all-gather = bf16[1024,22]{0,1:T(8,128)(2,1)S(1)} all-gather(bf16[128,22]{0,1:T(8,128)(2,1)S(1)} %fusion.28), channel_id=2, replica_groups=mesh['ra_0'=8,'ra_1'=4,'cb'=8] {'ra_0'}, dimensions={0}, use_global_device_ids=true | all-gather | bytes 50688 | tf_op jit(solution)/shard_map/all_gather | solution.py:32
  143.0 9.7 %all-gather.1 = bf16[32,128,22]{1,0,2:T(8,128)(2,1)S(1)} all-gather(bf16[8,128,22]{1,0,2:T(8,128)(2,1)S(1)} %slice_bitcast_fusion.1), channel_id=3, replica_groups=mesh['ra_0'=8,'ra_1'=4,'cb'=8] {'ra_1'}, dimensions={0}, use_global_device_ids=true | all-gather | bytes 225280 | tf_op jit(solution)/shard_map/all_gather | solution.py:32
  153.0 0.9 copy-done.1
  154.0 30.3 %all-gather.2 = f32[1024,64]{0,1:T(8,128)S(1)} all-gather(f32[128,64]{0,1:T(8,128)S(1)} %fusion.10), channel_id=4, replica_groups=mesh['ra_0'=8,'ra_1'=4,'cb'=8] {'cb'}, dimensions={0}, use_global_device_ids=true | all-gather | bytes 294912 | tf_op jit(solution)/shard_map/all_gather | solution.py:44
  184.5 11.9 %all-reduce.12 = (f32[128]{0:T(128)S(1)}, f32[128]{0:T(128)S(1)}, f32[128]{0:T(128)S(1)}) all-reduce(f32[128]{0:T(128)S(1)} %get-tuple-element.6, f32[128]{0:T(128)S(1)} %get-tuple-element.5, f32[128]{0:T(128)S(1)} %get-tuple-element.7), channel_id=1, replica_groups=mesh['ra_0'=8,'ra_1'=4,'cb'=8] {'ra_0'}, use_global_device_ids=true, to_apply=%region_15.16 | all-reduce | flops 384 | bytes 3072 | tf_op jit(solution)/shard_map/psum | solution.py:48
  196.4 7.1 %all-reduce.13 = (f32[128]{0:T(128)S(1)}, f32[128]{0:T(128)S(1)}, f32[128]{0:T(128)S(1)}) all-reduce(f32[128]{0:T(128)S(1)} %get-tuple-element.8, f32[128]{0:T(128)S(1)} %get-tuple-element.9, f32[128]{0:T(128)S(1)} %get-tuple-element.10), channel_id=1, replica_groups=mesh['ra_0'=8,'ra_1'=4,'cb'=8] {'ra_1'}, use_global_device_ids=true, to_apply=%region_16.17 | all-reduce | flops 384 | bytes 3072 | tf_op jit(solution)/shard_map/psum | solution.py:48
  203.6 1.0 fusion.6
  204.7 1.0 fusion.8
  205.7 34.0 %reduce-scatter.27.cloned.1.call-done = f32[128,88]{0,1:T(8,128)} async-done(((f32[128,704]{0,1:T(8,128)}), f32[128,88]{0,1:T(8,128)}) %reduce-scatter.27.cloned.1.call-update) | async-done | bytes 45072
  239.8 38.5 %reduce-scatter.25.cloned.1.call-done = f32[128,88]{0,1:T(8,128)} async-done(((f32[128,704]{0,1:T(8,128)}), f32[128,88]{0,1:T(8,128)}) %reduce-scatter.25.cloned.1.call-update) | async-done | bytes 45072
  278.2 9.9 %fusion.31 = (f32[128,32]{0,1:T(8,128)S(1)}, f32[128,32]{0,1:T(8,128)S(1)}) fusion(f32[128,88]{0,1:T(8,128)} %reduce-scatter.27.cloned.1.call-done, f32[128,88]{0,1:T(8,128)} %reduce-scatter.25.cloned.1.call-done), kind=kCustom, calls=%all-reduce-scatter.4 | all-reduce-scatter fusion | flops 32769 | bytes 123904
  288.1 1.3 collective-permute-start.2
  289.4 2.8 collective-permute-start.3
  293.2 18.5 %all-gather.3 = bf16[1024,22]{0,1:T(8,128)(2,1)S(1)} all-gather(bf16[128,22]{0,1:T(8,128)(2,1)S(1)} %fusion.27), channel_id=5, replica_groups=mesh['ra_0'=8,'ra_1'=4,'cb'=8] {'ra_0'}, dimensions={0}, use_global_device_ids=true | all-gather | bytes 50688 | tf_op jit(solution)/shard_map/all_gather | solution.py:32
  311.7 9.6 %all-gather.4 = bf16[32,128,22]{1,0,2:T(8,128)(2,1)S(1)} all-gather(bf16[8,128,22]{1,0,2:T(8,128)(2,1)S(1)} %slice_bitcast_fusion), channel_id=6, replica_groups=mesh['ra_0'=8,'ra_1'=4,'cb'=8] {'ra_1'}, dimensions={0}, use_global_device_ids=true | all-gather | bytes 225280 | tf_op jit(solution)/shard_map/all_gather | solution.py:32
  321.6 30.4 %all-gather.5 = f32[1024,64]{0,1:T(8,128)S(1)} all-gather(f32[128,64]{0,1:T(8,128)S(1)} %fusion.4), channel_id=7, replica_groups=mesh['ra_0'=8,'ra_1'=4,'cb'=8] {'cb'}, dimensions={0}, use_global_device_ids=true | all-gather | bytes 294912 | tf_op jit(solution)/shard_map/all_gather | solution.py:44
  352.2 11.8 %psum.78 = f32[128]{0:T(128)S(1)} all-reduce(f32[128]{0:T(128)S(1)} %multiply_reduce_fusion), channel_id=1, replica_groups=mesh['ra_0'=8,'ra_1'=4,'cb'=8] {'ra_0'}, use_global_device_ids=true, to_apply=%region_23.24 | all-reduce | flops 128 | bytes 1024 | tf_op jit(solution)/shard_map/psum | solution.py:48
  364.0 7.9 %psum.79 = f32[128]{0:T(128)S(1)} all-reduce(f32[128]{0:T(128)S(1)} %psum.78), channel_id=1, replica_groups=mesh['ra_0'=8,'ra_1'=4,'cb'=8] {'ra_1'}, use_global_device_ids=true, to_apply=%region_24.25 | all-reduce | flops 128 | bytes 1024 | tf_op jit(solution)/shard_map/psum | solution.py:48
  371.9 0.7 add_convert_fusion
  (56 shorter events, 3.3 us)
Async XLA Ops:
  6.5 27.5 %copy-start = (bf16[128,64]{0,1:T(8,128)(2,1)S(1)}, bf16[128,64]{0,1:T(8,128)(2,1)}, u32[]{:S(2)}) copy-start(bf16[128,64]{0,1:T(8,128)(2,1)} %param.6) | copy-start | bytes 49156
  6.5 62.9 %reduce-scatter.23.cloned.1.call-start = ((), (), s32[]{:S(2)}) async-start(), calls=%async_computation.5 | async-start | bytes 405504
  33.4 0.7 copy-start.4
  35.9 0.9 copy-start.3
  36.0 72.2 %reduce-scatter.21.cloned.1.call-start = ((), (), s32[]{:S(2)}) async-start(), calls=%async_computation.4 | async-start | bytes 405504
  37.9 201.8 %reduce-scatter.27.cloned.1.call-start = ((), (), s32[]{:S(2)}) async-start(), calls=%async_computation.7 | async-start | bytes 405504
  118.3 4.1 %copy-start.5 = (f32[2,64]{1,0:T(2,128)S(1)}, f32[2,64]{1,0:T(2,128)}, u32[]{:S(2)}) copy-start(f32[2,64]{1,0:T(2,128)} %param.8) | copy-start | bytes 1540
  118.4 6.0 %collective-permute-start = (f32[128,30]{0,1:T(8,128)S(1)}, f32[128,30]{0,1:T(8,128)S(1)}, u32[]{:S(2)}, u32[]{:S(2)}) collective-permute-start(f32[128,30]{0,1:T(8,128)S(1)} %slice.40), channel_id=1, source_target_pairs={{0,8},{8,16},{16,24},{1,9},{9,17},{17,25},{2,10},{10,18},{18,26},{... | collective-permute-start | bytes 46088
  119.7 4.9 %collective-permute-start.1 = (f32[128,30]{0,1:T(8,128)S(1)}, f32[128,30]{0,1:T(8,128)S(1)}, u32[]{:S(2)}, u32[]{:S(2)}) collective-permute-start(f32[128,30]{0,1:T(8,128)S(1)} %slice.41), channel_id=1, source_target_pairs={{0,8},{8,16},{16,24},{1,9},{9,17},{17,25},{2,10},{10,18},{18,26},{... | collective-permute-start | bytes 46088
  122.5 0.7 copy-start.6
  152.9 0.9 copy-start.1
  184.3 19.2 %copy-start.2 = (bf16[2,64,704]{2,1,0:T(8,128)(2,1)S(1)}, bf16[2,64,704]{2,1,0:T(8,128)(2,1)}, u32[]{:S(2)}) copy-start(bf16[2,64,704]{2,1,0:T(8,128)(2,1)} %param.10) | copy-start | bytes 540676
  204.6 73.6 %reduce-scatter.25.cloned.1.call-start = ((), (), s32[]{:S(2)}) async-start(), calls=%async_computation.6 | async-start | bytes 405504
  288.1 4.1 %collective-permute-start.2 = (f32[128,30]{0,1:T(8,128)S(1)}, f32[128,30]{0,1:T(8,128)S(1)}, u32[]{:S(2)}, u32[]{:S(2)}) collective-permute-start(f32[128,30]{0,1:T(8,128)S(1)} %slice.42), channel_id=1, source_target_pairs={{0,8},{8,16},{16,24},{1,9},{9,17},{17,25},{2,10},{10,18},{18,26},{... | collective-permute-start | bytes 46088
  289.4 3.6 collective-permute-start.3
Sparse Core Ops, SparseCore 0:
  36.1 33.3 reduce-scatter.22
  72.0 36.1 reduce-scatter.20
  204.7 34.9 reduce-scatter.26
  242.1 36.0 reduce-scatter.24
where the time goes:
time: 384 us; the launch traced here: 379 us
  blocking collectives  201 us (52%)
  waiting for transfers between devices  143 us (37%)
  between operations  14.1 us (4%)
  starting transfers between devices  8.25 us (2%)
  matrix products  5.3 us (1%)
  local copies, waits for them, and re-layouts  4.83 us (1%)
    unnamed x12, waiting for transfers between devices  143 us
    psum x6, blocking collectives, by_axis(): return functools.reduce(lax.psum, axes, array)  64.7 us
    all_gather x2, blocking collectives, gathered_total(): return lax.all_gather(array, axis).sum(0)  60.7 us
    all_gather x4, blocking collectives, gather_in_order(): tiles = lax.all_gather(tiles, axes[k])  55.9 us
    unnamed x2, blocking collectives  20 us
    unnamed x8, starting transfers between devices  8.25 us
  transfers between devices with their start and end apart: 8, of which 5 were waited for; matrix products, arithmetic and copies ran while one was open for 1% of the time, Pallas kernels for 0%

commit v1 on v0

v1 whole, which is shorter than its diff:
```python
import functools

import jax
import jax.numpy as jnp
from jax import lax
from jax.experimental import pallas as pl
from jax.experimental.pallas import tpu as pltpu
from jax.sharding import PartitionSpec as P

MESH = pl.DeviceIdType.MESH
F32, BF16 = jnp.float32, jnp.bfloat16

D = 2048
EPSILON = 1e-06
RESIDUAL = 0.25
NY, NZ, NC = 4, 8, 8
NR = NY * NZ
TOKENS = 128
ROWS = TOKENS // NZ
FEATURES = D // NR
UNITS = 704
MAIN, REST = 128, 48
STAT = 96


def terms(value):
    high = value.astype(BF16).astype(F32)
    left = value - high
    middle = left.astype(BF16).astype(F32)
    return [high, middle, left - middle]


def joined(tile, lane):
    return tile[:, lane : lane + 1] + tile[:, lane + 1 : lane + 2] + tile[:, lane + 2 : lane + 3]


def silu(value):
    return value / (1.0 + jnp.exp(-value))


def kernel(
    tokens_hbm, pre_hbm, post_hbm, gate_hbm, up_hbm, down_hbm, out_ref,
    tokens_v, gains_v, gate_v, up_v, down_v, wide_v, tall_v,
    sent_v, got_v, mine_v, hidden_v, part_v, parts_v, norm_v, norms_v,
    load_sem, send_sem, recv_sem,
):
    r, c = lax.axis_index("ra"), lax.axis_index("cb")
    z, y = r // NY, r % NY

    def plane(k):
        other = k + 1
        dz, dy = other // NY, other % NY
        there_z, there_y = lax.rem(z + dz, NZ), lax.rem(y + dy, NY)
        return other, there_z, there_y, there_z * NY + there_y

    barrier = pltpu.get_barrier_semaphore()

    def greet_plane(k, carry):
        pl.semaphore_signal(barrier, inc=1, device_id={"ra": plane(k)[3]}, device_id_type=MESH)
        return carry

    def greet_row(k, carry):
        pl.semaphore_signal(barrier, inc=1, device_id={"cb": lax.rem(c + k + 1, NC)}, device_id_type=MESH)
        return carry

    lax.fori_loop(0, NR - 1, greet_plane, 0)
    lax.fori_loop(0, NC - 1, greet_row, 0)

    loads = [
        pltpu.make_async_copy(tokens_hbm, tokens_v, load_sem.at[0]),
        pltpu.make_async_copy(pre_hbm, gains_v.at[0], load_sem.at[1]),
        pltpu.make_async_copy(post_hbm, gains_v.at[1], load_sem.at[2]),
        pltpu.make_async_copy(gate_hbm, gate_v, load_sem.at[3]),
        pltpu.make_async_copy(up_hbm, up_v, load_sem.at[4]),
        pltpu.make_async_copy(down_hbm, down_v, load_sem.at[5]),
    ]
    for load in loads:
        load.start()
    for load in loads:
        load.wait()

    def square(value):
        rows, lanes = value.shape
        if rows < 128:
            value = jnp.concatenate([value, jnp.zeros((128 - rows, lanes), F32)], axis=0)
        if lanes < 128:
            value = jnp.concatenate([value, jnp.zeros((value.shape[0], 128 - lanes), F32)], axis=1)
        return value.T

    row = lax.broadcasted_iota(jnp.int32, (64, 128), 0)
    lane = lax.broadcasted_iota(jnp.int32, (64, 128), 1)
    passing = jnp.where(row == lane - STAT, 1.0, 0.0).astype(BF16)
    nothing = jnp.zeros((64, 128), BF16)
    for l in range(2):
        gate_tail = gate_v[l, :, 512:704].astype(F32)
        up_tail = up_v[l, :, 512:704].astype(F32)
        pad = jnp.zeros((64, 64), F32)
        gate_tail = jnp.concatenate([gate_tail, pad], axis=1)
        up_tail = jnp.concatenate([up_tail, pad], axis=1)
        for q in range(NY):
            wide_v[l, 0:64, q * 384 : q * 384 + 128] = gate_v[l, :, q * 128 : q * 128 + 128]
            wide_v[l, 0:64, q * 384 + 128 : q * 384 + 256] = up_v[l, :, q * 128 : q * 128 + 128]
            gate_rest = pltpu.roll(gate_tail, (256 - REST * q) % 256, 1)[:, 0:128] if q else gate_tail[:, 0:128]
            up_rest = pltpu.roll(up_tail, (256 + REST - REST * q) % 256, 1)[:, 0:128] if q != 1 else up_tail[:, 0:128]
            rest = jnp.where(lane < REST, gate_rest, jnp.where(lane < 2 * REST, up_rest, 0.0))
            wide_v[l, 0:64, q * 384 + 256 : q * 384 + 384] = rest.astype(BF16)
            wide_v[l, 64:128, q * 384 : q * 384 + 128] = nothing
            wide_v[l, 64:128, q * 384 + 128 : q * 384 + 256] = nothing
            wide_v[l, 64:128, q * 384 + 256 : q * 384 + 384] = passing

    pick_row = lax.broadcasted_iota(jnp.int32, (16, 128), 0)
    pick_lane = lax.broadcasted_iota(jnp.int32, (16, 128), 1)
    pick = jnp.where((pick_row == 0) & (pick_lane >= REST) & (pick_lane < REST + 3), 1.0, 0.0).astype(BF16)
    for l in range(2):
        for q in range(NY):
            main = down_v[l, q * MAIN : q * MAIN + MAIN, :].astype(F32)
            rest = down_v[l, 512 + q * REST : 512 + q * REST + REST, :].astype(F32)
            tall_v[l, 0:64, q * 256 : q * 256 + 128] = square(main)[0:64].astype(BF16)
            tall_v[l, 0:64, q * 256 + 128 : q * 256 + 256] = square(rest)[0:64].astype(BF16)
            tall_v[l, 64:80, q * 256 : q * 256 + 128] = jnp.zeros((16, 128), BF16)
            tall_v[l, 64:80, q * 256 + 128 : q * 256 + 256] = pick if q == 0 else jnp.zeros((16, 128), BF16)

    stream0 = square(tokens_v[...].astype(F32))[0:64]
    gains = [square(jnp.concatenate([gains_v[i], jnp.zeros((6, 64), F32)], axis=0))[0:64] for i in range(2)]
    pre = [gains[0][:, l : l + 1] for l in range(2)]
    post = [gains[1][:, l : l + 1] for l in range(2)]

    def multiply(l, slot, features, statistics):
        lines = [t for s in statistics for t in terms(s)]
        lines = jnp.concatenate(lines + [jnp.zeros((64 - len(lines), 128), F32)], axis=0) if lines else jnp.zeros((64, 128), F32)
        left = jnp.concatenate([features, lines], axis=0).T
        high = left.astype(BF16)
        low = (left - high.astype(F32)).astype(BF16)
        for q in range(NY):
            wide = wide_v[l, :, q * 384 : q * 384 + 384]
            part = jnp.dot(high, wide, preferred_element_type=F32) + jnp.dot(low, wide, preferred_element_type=F32)
            sent_v[slot, :, q] = part.reshape(NZ, ROWS, 384).astype(BF16)

    def scatter(slot):
        def step(k, carry):
            other, tz, ty, there = plane(k)
            pltpu.make_async_remote_copy(
                src_ref=sent_v.at[slot, tz, ty],
                dst_ref=got_v.at[slot, other],
                send_sem=send_sem.at[slot],
                recv_sem=recv_sem.at[slot],
                device_id={"ra": there},
                device_id_type=MESH,
            ).start()
            return carry

        lax.fori_loop(0, NR - 1, step, 0)

    def all_of(ref, sem):
        pltpu.make_async_copy(ref, ref, sem).wait()

    def total(slot):
        all_of(got_v.at[slot, pl.ds(1, NR - 1)], recv_sem.at[slot])
        acc = sent_v[slot, z, y].astype(F32)
        for k in range(1, NR):
            acc = acc + got_v[slot, k].astype(F32)
        return acc

    small_lane = lax.broadcasted_iota(jnp.int32, (ROWS, 128), 1)

    def activate(main_gate, main_up, rest_tile, extra):
        main = silu(main_gate) * main_up
        rest = silu(rest_tile) * pltpu.roll(rest_tile, 128 - REST, 1)
        rest = jnp.where(small_lane < REST, rest, 0.0)
        if extra is not None:
            for i, term in enumerate(terms(extra)):
                rest = jnp.where(small_lane == REST + i, term, rest)
        return main.astype(BF16), rest.astype(BF16)

    def broadcast_hidden(l, pair):
        mine_v[l, :, 0:128] = pair[0]
        mine_v[l, :, 128:256] = pair[1]

        def step(k, carry):
            pltpu.make_async_remote_copy(
                src_ref=mine_v.at[l],
                dst_ref=hidden_v.at[l, y, z],
                send_sem=send_sem.at[3 + l],
                recv_sem=recv_sem.at[3 + l],
                device_id={"ra": plane(k)[3]},
                device_id_type=MESH,
            ).start()
            return carry

        lax.fori_loop(0, NR - 1, step, 0)
        hidden_v[l, y, z, :, 0:128] = pair[0]
        hidden_v[l, y, z, :, 128:256] = pair[1]

    def project(l):
        all_of(got_v.at[0, pl.ds(1, NR - 1), :, pl.ds(0, 256)], recv_sem.at[3 + l])
        acc = jnp.zeros((80, 128), F32)
        for q in range(NY):
            right = hidden_v[l, q].reshape(TOKENS, 256)
            acc = acc + lax.dot_general(
                tall_v[l, :, q * 256 : q * 256 + 256], right, (((1,), (1,)), ((), ())), preferred_element_type=F32
            )
        return acc

    def branch_total(l, part):
        part_v[l] = part.astype(BF16)

        def step(k, carry):
            pltpu.make_async_remote_copy(
                src_ref=part_v.at[l],
                dst_ref=parts_v.at[l, c],
                send_sem=send_sem.at[5 + l],
                recv_sem=recv_sem.at[5 + l],
                device_id={"cb": lax.rem(c + k + 1, NC)},
                device_id_type=MESH,
            ).start()
            return carry

        lax.fori_loop(0, NC - 1, step, 0)
        parts_v[l, c] = part.astype(BF16)
        all_of(parts_v.at[l, pl.ds(0, NC - 1)], recv_sem.at[5 + l])
        acc = parts_v[l, 0].astype(F32)
        for k in range(1, NC):
            acc = acc + parts_v[l, k].astype(F32)
        return acc

    def over_features(value):
        return jnp.sum(value, axis=0, keepdims=True)

    multiply(0, 0, stream0 * pre[0], [over_features(stream0 * stream0)])
    pl.semaphore_wait(barrier, NR - 1 + NC - 1)
    scatter(0)
    multiply(1, 1, stream0 * pre[1], [])
    acc = total(0)
    squares = joined(acc[:, 256:384], STAT)
    scale = lax.rsqrt(squares / D + EPSILON)
    acc = acc * scale
    broadcast_hidden(0, activate(acc[:, 0:128], acc[:, 128:256], acc[:, 256:384], None))
    scatter(1)
    branch = branch_total(0, project(0)[0:64])
    gained = branch * post[0]

    multiply(1, 2, gained * pre[1], [over_features(branch * branch), over_features(gained * gained), over_features(stream0 * gained)])
    scatter(2)
    early = total(1)
    acc = total(2)
    rest = acc[:, 256:384]
    scale_out = lax.rsqrt(joined(rest, STAT) / D + EPSILON)
    squares = (
        RESIDUAL * RESIDUAL * squares
        + 2.0 * RESIDUAL * scale_out * joined(rest, STAT + 6)
        + scale_out * scale_out * joined(rest, STAT + 3)
    )
    scale = lax.rsqrt(squares / D + EPSILON)
    acc = scale * (RESIDUAL * early + scale_out * acc)
    broadcast_hidden(1, activate(acc[:, 0:128], acc[:, 128:256], acc[:, 256:384], scale_out))
    both = project(1)
    stream1 = RESIDUAL * stream0 + gained * both[64:65]
    branch = branch_total(1, both[0:64])
    norm_v[...] = over_features(branch * branch)

    def tell(k, carry):
        pltpu.make_async_remote_copy(
            src_ref=norm_v,
            dst_ref=norms_v.at[r],
            send_sem=send_sem.at[7],
            recv_sem=recv_sem.at[7],
            device_id={"ra": plane(k)[3]},
            device_id_type=MESH,
        ).start()
        return carry

    lax.fori_loop(0, NR - 1, tell, 0)
    norms_v[r] = norm_v[...]
    all_of(norms_v.at[pl.ds(0, NR - 1)], recv_sem.at[7])
    norm = norms_v[0]
    for k in range(1, NR):
        norm = norm + norms_v[k]
    scale_out = lax.rsqrt(norm / D + EPSILON)
    stream2 = RESIDUAL * stream1 + branch * post[1] * scale_out
    out_ref[...] = square(stream2)[:, 0:64].astype(BF16)

    for slot in range(3):
        all_of(got_v.at[slot, pl.ds(1, NR - 1)], send_sem.at[slot])
    for l in range(2):
        all_of(got_v.at[0, pl.ds(1, NR - 1), :, pl.ds(0, 256)], send_sem.at[3 + l])
        all_of(parts_v.at[l, pl.ds(0, NC - 1)], send_sem.at[5 + l])
    all_of(norms_v.at[pl.ds(0, NR - 1)], send_sem.at[7])


def per_device(tokens, pre_gain, post_gain, gate_weight, up_weight, down_weight):
    return pl.pallas_call(
        kernel,
        out_shape=jax.ShapeDtypeStruct((TOKENS, FEATURES), BF16),
        in_specs=[pl.BlockSpec(memory_space=pl.ANY)] * 6,
        out_specs=pl.BlockSpec(memory_space=pltpu.VMEM),
        scratch_shapes=[
            pltpu.VMEM((TOKENS, FEATURES), BF16),
            pltpu.VMEM((2, 2, FEATURES), F32),
            pltpu.VMEM((2, FEATURES, UNITS), BF16),
            pltpu.VMEM((2, FEATURES, UNITS), BF16),
            pltpu.VMEM((2, UNITS, FEATURES), BF16),
            pltpu.VMEM((2, 128, NY * 384), BF16),
            pltpu.VMEM((2, 80, NY * 256), BF16),
            pltpu.VMEM((3, NZ, NY, ROWS, 384), BF16),
            pltpu.VMEM((3, NR, ROWS, 384), BF16),
            pltpu.VMEM((2, ROWS, 256), BF16),
            pltpu.VMEM((2, NY, NZ, ROWS, 256), BF16),
            pltpu.VMEM((2, FEATURES, TOKENS), BF16),
            pltpu.VMEM((2, NC, FEATURES, TOKENS), BF16),
            pltpu.VMEM((1, TOKENS), F32),
            pltpu.VMEM((NR, 1, TOKENS), F32),
            pltpu.SemaphoreType.DMA((6,)),
            pltpu.SemaphoreType.DMA((8,)),
            pltpu.SemaphoreType.DMA((8,)),
        ],
        compiler_params=pltpu.CompilerParams(collective_id=0, has_side_effects=True),
    )(tokens, pre_gain, post_gain, gate_weight, up_weight, down_weight)


def solution(mesh):
    return jax.shard_map(
        per_device,
        mesh=mesh,
        in_specs=(
            P(None, "ra"),
            P(None, "ra"),
            P(None, "ra"),
            P(None, "ra", "cb"),
            P(None, "ra", "cb"),
            P(None, "cb", "ra"),
        ),
        out_specs=P(None, "ra"),
        check_vma=False,
    )
```

time: 384 us -> 80 us (0.21); the launches traced: 379 us -> 79.8 us
  blocking collectives: 201 us -> 0 us
  waiting for transfers between devices: 143 us -> 0 us
  Pallas kernels: 0 us -> 75.1 us
  between operations: 14.1 us -> 0.01 us
  starting transfers between devices: 8.25 us -> 0 us
  matrix products: 5.3 us -> 0 us
    unnamed x12 -> x0, waiting for transfers between devices: 143 us -> none
    all_gather x6 -> x0, blocking collectives: 117 us -> none  [the longest x2 60.7 us: gathered_total(): return lax.all_gather(array, axis).sum(0)]
    pallas_call x0 -> x1, Pallas kernels: none -> 75.1 us  [per_device(): pl.pallas_call(kernel, out_shape=jax.ShapeDtypeStruct((TOKENS, FEATURES),...]
    psum x6 -> x0, blocking collectives: 64.7 us -> none  [by_axis(): return functools.reduce(lax.psum, axes, array)]
    unnamed x2 -> x0, blocking collectives: 20 us -> none
    unnamed x8 -> x0, starting transfers between devices: 8.25 us -> none
    dot_general x6 -> x0, matrix products: 5.3 us -> none  [the longest x2 2.93 us: project(): up_part = jnp.dot(normed, up_block, preferred_element_type=jnp.float32)]
  transfers between devices with their start and end apart: 8 -> 0, of which waited for: 5 -> 0; matrix products, arithmetic and copies ran while one was open for 1% -> 0% of each run, Pallas kernels for 0% -> 0%
where the time goes in v1:
time: 80 us; the launch traced here: 79.8 us
  Pallas kernels  75.1 us (94%)
  local copies, waits for them, and re-layouts  4.7 us (6%)
    pallas_call x1, Pallas kernels, per_device(): pl.pallas_call(kernel, out_shape=jax.ShapeDtypeStruct((TOKENS, FEATURES),...  75.1 us
    unnamed x2, local copies, waits for them, and re-layouts  3.25 us

profile of v1, /device:TPU:1, one launch (start us, length us, event | category | flops | bytes accessed | tf_op | source)
XLA Modules:
  0.0 79.8 jit_solution(13702069417786738550)
XLA Ops:
  0.0 1.4 %copy.7.tokens_hbm = bf16[128,64]{1,0:T(8,128)(2,1)} copy(bf16[128,64]{0,1:T(8,128)(2,1)} %param.6) | data formatting | bytes 32768 | tf_op args[0]
  1.4 1.8 %copy.8.down_hbm = bf16[2,704,64]{2,1,0:T(8,128)(2,1)} copy(bf16[2,704,64]{1,2,0:T(8,128)(2,1)} %param.11) | data formatting | bytes 360448 | tf_op args[5]
  3.3 75.1 %shard_map.64 = bf16[128,64]{1,0:T(8,128)(2,1)} custom-call(bf16[128,64]{1,0:T(8,128)(2,1)} %copy.7.tokens_hbm, f32[2,64]{1,0:T(2,128)} %pre_hbm.1, f32[2,64]{1,0:T(2,128)} %post_hbm.1, bf16[2,64,704]{2,1,0:T(8,128)(2,1)} %gate_hbm.1, bf16[2,64,704]{2,1,0:T(8,128)(2,1)} %up_hbm.1, bf16[2,704,64]{2,1,0:T(8,128)(2,1)} %copy.8.down_hbm), custom_call_target="tpu_custom_call" | custom-call | tf_op jit(solution)/shard_map/pallas_call | solution.py:291
  78.3 1.4 %copy.9 = bf16[128,64]{0,1:T(8,128)(2,1)} copy(bf16[128,64]{1,0:T(8,128)(2,1)} %shard_map.64) | data formatting | bytes 32768 | tf_op jit(solution)/shard_map/pallas_call | solution.py:291

commit v2 on v0

v2 whole, which is shorter than its diff:
```python
import jax
import jax.numpy as jnp
from jax import lax
from jax.experimental import pallas as pl
from jax.experimental.pallas import tpu as pltpu
from jax.sharding import PartitionSpec as P

MESH = pl.DeviceIdType.MESH
F32, BF16 = jnp.float32, jnp.bfloat16

D = 2048
EPSILON = 1e-06
RESIDUAL = 0.25
NY, NZ, NC = 4, 8, 8
NR = NY * NZ
TOKENS = 128
ROWS = TOKENS // NZ
FEATURES = D // NR
UNITS = 704
REST = 48
STAT = 96
Z_ORDER = (4, 3, 5, 2, 6, 1, 7)
Y_ORDER = (2, 1, 3)


def terms(value):
    high = value.astype(BF16).astype(F32)
    left = value - high
    middle = left.astype(BF16).astype(F32)
    return [high, middle, left - middle]


def joined(tile, lane):
    return tile[:, lane : lane + 1] + tile[:, lane + 1 : lane + 2] + tile[:, lane + 2 : lane + 3]


def silu(value):
    return value / (1.0 + jnp.exp(-value))


def over_features(value):
    return jnp.sum(value, axis=0, keepdims=True)


def all_of(ref, sem):
    pltpu.make_async_copy(ref, ref, sem).wait()


def kernel(
    tokens_hbm, pre_hbm, post_hbm, gate_hbm, up_hbm, down_hbm, out_ref,
    tokens_v, gains_v, gate_v, up_v, down_v, tokens4_v, gains4_v,
    wide_from_v, wide_v, tall_from_v, tall_v,
    square_v, squares_v, sent_v, got_v, mine_v, hidden_v,
    piece_v, own_v, pieces_v, part_v, parts_v, block_v, branch_v, stream_v, gained_v, norm_v, norms_v,
    load_sem, send_sem, recv_sem,
):
    r, c = lax.axis_index("ra"), lax.axis_index("cb")
    z, y = r // NY, r % NY
    pending = []

    def to_z(dz):
        there = lax.rem(z + dz, NZ)
        return there, {"ra": there * NY + y}

    def to_y(dy):
        there = lax.rem(y + dy, NY)
        return there, {"ra": z * NY + there}

    def to_c(dc):
        there = lax.rem(c + dc, NC)
        return there, {"cb": there}

    def push(src, dst, which, device):
        pltpu.make_async_remote_copy(
            src_ref=src, dst_ref=dst, send_sem=send_sem.at[which], recv_sem=recv_sem.at[which],
            device_id=device, device_id_type=MESH,
        ).start()

    barrier = pltpu.get_barrier_semaphore()
    for device in [to_z(k)[1] for k in range(1, NZ)] + [to_y(k)[1] for k in range(1, NY)] + [to_c(k)[1] for k in range(1, NC)]:
        pl.semaphore_signal(barrier, inc=1, device_id=device, device_id_type=MESH)

    loads = [
        pltpu.make_async_copy(gate_hbm, gate_v, load_sem.at[0]),
        pltpu.make_async_copy(up_hbm, up_v, load_sem.at[1]),
        pltpu.make_async_copy(tokens_hbm, tokens_v, load_sem.at[2]),
        pltpu.make_async_copy(pre_hbm, gains_v.at[0], load_sem.at[3]),
        pltpu.make_async_copy(post_hbm, gains_v.at[1], load_sem.at[4]),
        pltpu.make_async_copy(down_hbm, down_v, load_sem.at[5]),
    ]
    for load in loads:
        load.start()

    lane64 = lax.broadcasted_iota(jnp.int32, (FEATURES, 128), 1)

    def tail(ref, l):
        return jnp.concatenate([ref[l, :, 512:704].astype(F32), jnp.zeros((FEATURES, 64), F32)], axis=1)

    def shifted(value, lanes):
        lanes = lanes % 256
        return pltpu.roll(value, lanes, 1)[:, 0:128] if lanes else value[:, 0:128]

    def arrange_wide(l):
        gate_tail, up_tail = tail(gate_v, l), tail(up_v, l)
        for q in range(NY):
            wide_from_v[l, q, :, 0:128] = gate_v[l, :, q * 128 : q * 128 + 128]
            wide_from_v[l, q, :, 128:256] = up_v[l, :, q * 128 : q * 128 + 128]
            rest = jnp.where(
                lane64 < REST, shifted(gate_tail, -REST * q), jnp.where(lane64 < 2 * REST, shifted(up_tail, REST - REST * q), 0.0)
            )
            wide_from_v[l, q, :, 256:384] = rest.astype(BF16)

    def arrange_tall(l):
        down_tail = tail(down_v, l)
        for q in range(NY):
            tall_from_v[l, q, :, 0:128] = down_v[l, :, q * 128 : q * 128 + 128]
            tall_from_v[l, q, :, 128:256] = jnp.where(lane64 < REST, shifted(down_tail, -REST * q), 0.0).astype(BF16)

    def exchange_wide(l):
        for dy in Y_ORDER:
            there, device = to_y(dy)
            push(wide_from_v.at[l, there], wide_v.at[l, y], l, device)
        wide_v[l, y] = wide_from_v[l, y]
        pending.append((wide_from_v.at[l, pl.ds(0, NY - 1)], send_sem.at[l]))

    def exchange_tall(l):
        for dy in Y_ORDER:
            there, device = to_y(dy)
            push(tall_from_v.at[l, there], tall_v.at[l, y], 2 + l, device)
        tall_v[l, y] = tall_from_v[l, y]
        pending.append((tall_from_v.at[l, pl.ds(0, NY - 1)], send_sem.at[2 + l]))

    loads[0].wait()
    loads[1].wait()
    arrange_wide(0)
    for load in loads[2:]:
        load.wait()
    pl.semaphore_wait(barrier, NZ - 1 + NY - 1 + NC - 1)


    for dy in Y_ORDER:
        push(tokens_v, tokens4_v.at[y], 4, to_y(dy)[1])
        push(gains_v, gains4_v.at[y], 5, to_y(dy)[1])
    tokens4_v[y] = tokens_v[...]
    gains4_v[y] = gains_v[...]
    pending.append((tokens4_v.at[pl.ds(0, NY - 1)], send_sem.at[4]))
    pending.append((gains4_v.at[pl.ds(0, NY - 1)], send_sem.at[5]))
    exchange_wide(0)

    arrange_tall(0)
    exchange_tall(0)
    all_of(tokens4_v.at[pl.ds(0, NY - 1)], recv_sem.at[4])
    stream0 = tokens4_v[...].reshape(NY * FEATURES, TOKENS).astype(F32)
    own_square = over_features(stream0 * stream0)
    square_v[...] = own_square
    for dz in Z_ORDER:
        push(square_v, squares_v.at[z], 6, to_z(dz)[1])
    squares_v[z] = own_square
    pending.append((squares_v.at[pl.ds(0, NZ - 1)], send_sem.at[6]))
    arrange_wide(1)
    exchange_wide(1)
    arrange_tall(1)
    exchange_tall(1)

    all_of(gains4_v.at[pl.ds(0, NY - 1)], recv_sem.at[5])
    lines = []
    for q in range(NY):
        lines += [gains4_v[q, 0], gains4_v[q, 1], jnp.zeros((4, FEATURES), F32)]
    lines = jnp.concatenate(lines + [jnp.zeros((128 - 8 * NY, FEATURES), F32)], axis=0)
    columns = jnp.concatenate([lines, jnp.zeros((128, 128 - FEATURES), F32)], axis=1).T[0:FEATURES]

    def gain(i):
        return jnp.concatenate([columns[:, 8 * q + i : 8 * q + i + 1] for q in range(NY)], axis=0)


    passing = jnp.where(
        lax.broadcasted_iota(jnp.int32, (128, 128), 0) == lax.broadcasted_iota(jnp.int32, (128, 128), 1) - STAT, 1.0, 0.0
    ).astype(BF16)

    def multiply(l, slot, features, statistics, exact):
        left = features.T
        high = left.astype(BF16)
        wide = wide_v[l].reshape(NY * FEATURES, 384)
        part = jnp.dot(high, wide, preferred_element_type=F32)
        if not exact:
            low = (left - high.astype(F32)).astype(BF16)
            part = part + jnp.dot(low, wide, preferred_element_type=F32)
        last = part[:, 256:384]
        if statistics:
            lines = [t for s in statistics for t in terms(s)]
            lines = jnp.concatenate(lines + [jnp.zeros((128 - len(lines), 128), F32)], axis=0)
            last = last + jnp.dot(lines.T.astype(BF16), passing, preferred_element_type=F32)
        sent_v[slot, :, :, 0:256] = part[:, 0:256].reshape(NZ, ROWS, 256).astype(BF16)
        sent_v[slot, :, :, 256:384] = last.reshape(NZ, ROWS, 128).astype(BF16)

    def scatter(slot):
        for dz in Z_ORDER:
            there, device = to_z(dz)
            push(sent_v.at[slot, there], got_v.at[slot, dz], 7 + slot, device)
        pending.append((got_v.at[slot, pl.ds(1, NZ - 1)], send_sem.at[7 + slot]))

    def total(slot):
        all_of(got_v.at[slot, pl.ds(1, NZ - 1)], recv_sem.at[7 + slot])
        acc = sent_v[slot, z].astype(F32)
        for k in range(1, NZ):
            acc = acc + got_v[slot, k].astype(F32)
        return acc

    small_lane = lax.broadcasted_iota(jnp.int32, (ROWS, 128), 1)

    def broadcast_hidden(l, acc, extra):
        rest = acc[:, 256:384]
        main = silu(acc[:, 0:128]) * acc[:, 128:256]
        rest = jnp.where(small_lane < REST, silu(rest) * pltpu.roll(rest, 128 - REST, 1), 0.0)
        if extra is not None:
            for i, term in enumerate(terms(extra)):
                rest = jnp.where(small_lane == REST + i, term, rest)
        both = jnp.concatenate([main, rest], axis=1).astype(BF16)
        mine_v[l] = both
        for dz in Z_ORDER:
            push(mine_v.at[l], hidden_v.at[l, z], 10 + l, to_z(dz)[1])
        hidden_v[l, z] = both
        pending.append((hidden_v.at[l, pl.ds(0, NZ - 1)], send_sem.at[10 + l]))

    def project(l):
        all_of(tall_v.at[l, pl.ds(0, NY - 1)], recv_sem.at[2 + l])
        all_of(hidden_v.at[l, pl.ds(0, NZ - 1)], recv_sem.at[10 + l])
        right = hidden_v[l].reshape(TOKENS, 256)
        return lax.dot_general(
            tall_v[l].reshape(NY * FEATURES, 256), right, (((1,), (1,)), ((), ())), preferred_element_type=F32
        )

    def branch_total(l, part):
        part = part.reshape(NY, FEATURES, TOKENS)
        piece_v[l] = part.astype(BF16)
        for dy in Y_ORDER:
            there, device = to_y(dy)
            push(piece_v.at[l, there], pieces_v.at[l, dy], 12 + l, device)
        own_v[...] = part
        pending.append((pieces_v.at[l, pl.ds(1, NY - 1)], send_sem.at[12 + l]))
        all_of(pieces_v.at[l, pl.ds(1, NY - 1)], recv_sem.at[12 + l])
        acc = own_v[y]
        for k in range(1, NY):
            acc = acc + pieces_v[l, k].astype(F32)
        rounded = acc.astype(BF16)
        part_v[l] = rounded
        for dc in range(1, NC):
            push(part_v.at[l], parts_v.at[l, c], 14 + l, to_c(dc)[1])
        parts_v[l, c] = rounded
        pending.append((parts_v.at[l, pl.ds(0, NC - 1)], send_sem.at[14 + l]))
        all_of(parts_v.at[l, pl.ds(0, NC - 1)], recv_sem.at[14 + l])
        acc = parts_v[l, 0].astype(F32)
        for k in range(1, NC):
            acc = acc + parts_v[l, k].astype(F32)
        return acc

    gains = [gain(i) for i in range(3)]
    all_of(squares_v.at[pl.ds(0, NZ - 1)], recv_sem.at[6])
    squares = squares_v[0]
    for k in range(1, NZ):
        squares = squares + squares_v[k]
    scale = lax.rsqrt(squares / D + EPSILON)
    all_of(wide_v.at[0, pl.ds(0, NY - 1)], recv_sem.at[0])
    multiply(0, 0, stream0 * scale * gains[0], [], True)
    scatter(0)
    all_of(wide_v.at[1, pl.ds(0, NY - 1)], recv_sem.at[1])
    multiply(1, 1, stream0 * gains[1], [own_square], False)
    acc = total(0)
    broadcast_hidden(0, acc, None)
    scatter(1)
    part = project(0)
    block = branch_total(0, part)
    block_v[...] = block
    for dy in Y_ORDER:
        push(block_v, branch_v.at[y], 16, to_y(dy)[1])
    branch_v[y] = block
    pending.append((branch_v.at[pl.ds(0, NY - 1)], send_sem.at[16]))
    all_of(branch_v.at[pl.ds(0, NY - 1)], recv_sem.at[16])
    branch = branch_v[...].reshape(NY * FEATURES, TOKENS)
    gained = branch * gains[2]

    multiply(1, 2, gained * gains[1], [over_features(branch * branch), over_features(gained * gained), over_features(stream0 * gained)], False)
    scatter(2)
    stream_v[...] = stream0.reshape(NY, FEATURES, TOKENS)
    gained_v[...] = gained.reshape(NY, FEATURES, TOKENS)
    early = total(1)
    acc = total(2)
    rest = acc[:, 256:384]
    scale_out = lax.rsqrt(joined(rest, STAT) / D + EPSILON)
    squares = (
        RESIDUAL * RESIDUAL * joined(early[:, 256:384], STAT)
        + 2.0 * RESIDUAL * scale_out * joined(rest, STAT + 6)
        + scale_out * scale_out * joined(rest, STAT + 3)
    )
    scale = lax.rsqrt(squares / D + EPSILON)
    acc = scale * (RESIDUAL * early + scale_out * acc)
    broadcast_hidden(1, acc, scale_out)
    part = project(1)
    picked = jnp.where(
        (lax.broadcasted_iota(jnp.int32, (16, 128), 1) >= REST) & (lax.broadcasted_iota(jnp.int32, (16, 128), 1) < REST + 3), 1.0, 0.0
    ).astype(BF16)
    scale_out = lax.dot_general(
        picked, hidden_v[1].reshape(TOKENS, 256)[:, 128:256], (((1,), (1,)), ((), ())), preferred_element_type=F32
    )[0:1]
    block = branch_total(1, part)
    norm = over_features(block * block)
    norm_v[...] = norm

    def tell(k, carry):
        other = k + 1
        there_z, there_y = lax.rem(z + other // NY, NZ), lax.rem(y + other % NY, NY)
        push(norm_v, norms_v.at[r], 17, {"ra": there_z * NY + there_y})
        return carry

    lax.fori_loop(0, NR - 1, tell, 0)
    norms_v[r] = norm
    pending.append((norms_v.at[pl.ds(0, NR - 1)], send_sem.at[17]))
    stream1 = RESIDUAL * stream_v[y] + gained_v[y] * scale_out
    post = jnp.zeros((FEATURES, 1), F32)
    for q in range(NY):
        post = jnp.where(y == q, columns[:, 8 * q + 3 : 8 * q + 4], post)
    all_of(norms_v.at[pl.ds(0, NR - 1)], recv_sem.at[17])
    norm = norms_v[0]
    for k in range(1, NR):
        norm = norm + norms_v[k]
    scale_out = lax.rsqrt(norm / D + EPSILON)
    out_ref[...] = (RESIDUAL * stream1 + block * post * scale_out).astype(BF16)
    for ref, sem in pending:
        all_of(ref, sem)


def per_device(tokens, pre_gain, post_gain, gate_weight, up_weight, down_weight):
    out = pl.pallas_call(
        kernel,
        out_shape=jax.ShapeDtypeStruct((FEATURES, TOKENS), BF16),
        in_specs=[pl.BlockSpec(memory_space=pl.ANY)] * 6,
        out_specs=pl.BlockSpec(memory_space=pltpu.VMEM),
        scratch_shapes=[
            pltpu.VMEM((FEATURES, TOKENS), BF16),
            pltpu.VMEM((2, 2, FEATURES), F32),
            pltpu.VMEM((2, FEATURES, UNITS), BF16),
            pltpu.VMEM((2, FEATURES, UNITS), BF16),
            pltpu.VMEM((2, FEATURES, UNITS), BF16),
            pltpu.VMEM((NY, FEATURES, TOKENS), BF16),
            pltpu.VMEM((NY, 2, 2, FEATURES), F32),
            pltpu.VMEM((2, NY, FEATURES, 384), BF16),
            pltpu.VMEM((2, NY, FEATURES, 384), BF16),
            pltpu.VMEM((2, NY, FEATURES, 256), BF16),
            pltpu.VMEM((2, NY, FEATURES, 256), BF16),
            pltpu.VMEM((1, TOKENS), F32),
            pltpu.VMEM((NZ, 1, TOKENS), F32),
            pltpu.VMEM((3, NZ, ROWS, 384), BF16),
            pltpu.VMEM((3, NZ, ROWS, 384), BF16),
            pltpu.VMEM((2, ROWS, 256), BF16),
            pltpu.VMEM((2, NZ, ROWS, 256), BF16),
            pltpu.VMEM((2, NY, FEATURES, TOKENS), BF16),
            pltpu.VMEM((NY, FEATURES, TOKENS), F32),
            pltpu.VMEM((2, NY, FEATURES, TOKENS), BF16),
            pltpu.VMEM((2, FEATURES, TOKENS), BF16),
            pltpu.VMEM((2, NC, FEATURES, TOKENS), BF16),
            pltpu.VMEM((FEATURES, TOKENS), F32),
            pltpu.VMEM((NY, FEATURES, TOKENS), F32),
            pltpu.VMEM((NY, FEATURES, TOKENS), F32),
            pltpu.VMEM((NY, FEATURES, TOKENS), F32),
            pltpu.VMEM((1, TOKENS), F32),
            pltpu.VMEM((NR, 1, TOKENS), F32),
            pltpu.SemaphoreType.DMA((6,)),
            pltpu.SemaphoreType.DMA((18,)),
            pltpu.SemaphoreType.DMA((18,)),
        ],
        compiler_params=pltpu.CompilerParams(collective_id=0, has_side_effects=True),
    )(tokens.T, pre_gain, post_gain, gate_weight, up_weight, down_weight.swapaxes(1, 2))
    return out.T


def solution(mesh):
    return jax.shard_map(
        per_device,
        mesh=mesh,
        in_specs=(
            P(None, "ra"),
            P(None, "ra"),
            P(None, "ra"),
            P(None, "ra", "cb"),
            P(None, "ra", "cb"),
            P(None, "cb", "ra"),
        ),
        out_specs=P(None, "ra"),
        check_vma=False,
    )
```

time: 384 us -> 66.8 us (0.17); the launches traced: 379 us -> 66.7 us
  blocking collectives: 201 us -> 0 us
  waiting for transfers between devices: 143 us -> 0 us
  Pallas kernels: 0 us -> 65.3 us
  between operations: 14.1 us -> 0.01 us
  starting transfers between devices: 8.25 us -> 0 us
  matrix products: 5.3 us -> 0 us
    unnamed x12 -> x0, waiting for transfers between devices: 143 us -> none
    all_gather x6 -> x0, blocking collectives: 117 us -> none  [the longest x2 60.7 us: gathered_total(): return lax.all_gather(array, axis).sum(0)]
    pallas_call x0 -> x1, Pallas kernels: none -> 65.3 us  [per_device(): pl.pallas_call(kernel, out_shape=jax.ShapeDtypeStruct((FEATURES, TOKENS),...]
    psum x6 -> x0, blocking collectives: 64.7 us -> none  [by_axis(): return functools.reduce(lax.psum, axes, array)]
    unnamed x2 -> x0, blocking collectives: 20 us -> none
    unnamed x8 -> x0, starting transfers between devices: 8.25 us -> none
    dot_general x6 -> x0, matrix products: 5.3 us -> none  [the longest x2 2.93 us: project(): up_part = jnp.dot(normed, up_block, preferred_element_type=jnp.float32)]
  transfers between devices with their start and end apart: 8 -> 0, of which waited for: 5 -> 0; matrix products, arithmetic and copies ran while one was open for 1% -> 0% of each run, Pallas kernels for 0% -> 0%
where the time goes in v2:
time: 66.8 us; the launch traced here: 66.7 us
  Pallas kernels  65.3 us (98%)
  local copies, waits for them, and re-layouts  1.32 us (2%)
    pallas_call x1, Pallas kernels, per_device(): pl.pallas_call(kernel, out_shape=jax.ShapeDtypeStruct((FEATURES, TOKENS),...  65.3 us

profile of v2, /device:TPU:1, one launch (start us, length us, event | category | flops | bytes accessed | tf_op | source)
XLA Modules:
  0.0 66.7 jit_solution(7327074549087744637)
XLA Ops:
  0.0 65.3 %shard_map.64 = bf16[64,128]{1,0:T(8,128)(2,1)} custom-call(bf16[64,128]{1,0:T(8,128)(2,1)} %bitcast.5, f32[2,64]{1,0:T(2,128)} %pre_hbm.1, f32[2,64]{1,0:T(2,128)} %post_hbm.1, bf16[2,64,704]{2,1,0:T(8,128)(2,1)} %gate_hbm.1, bf16[2,64,704]{2,1,0:T(8,128)(2,1)} %up_hbm.1, bf16[2,64,704]{2,1,0:T(8,128)(2,1)} %bitcast.3), custom_call_target="tpu_custom_call" | custom-call | tf_op jit(solution)/shard_map/pallas_call | solution.py:333
  65.3 1.3 %copy.8 = bf16[128,64]{0,1:T(8,128)(2,1)} copy(bf16[128,64]{0,1:T(8,128)(2,1)} %bitcast.4) | data formatting | bytes 32768

commit v3 on v2

--- a/solution.py
+++ b/solution.py
@@ -50,8 +50,8 @@
     tokens_hbm, pre_hbm, post_hbm, gate_hbm, up_hbm, down_hbm, out_ref,
     tokens_v, gains_v, gate_v, up_v, down_v, tokens4_v, gains4_v,
     wide_from_v, wide_v, tall_from_v, tall_v,
-    square_v, squares_v, sent_v, got_v, mine_v, hidden_v,
-    piece_v, own_v, pieces_v, part_v, parts_v, block_v, branch_v, stream_v, gained_v, norm_v, norms_v,
+    sent_v, got_v, mine_v, hidden_v,
+    piece_v, own_v, pieces_v, part_v, parts_v, block_v, branch_v, shared_v, shares_v, stream_v, gained_v, norm_v, norms_v,
     load_sem, send_sem, recv_sem,
 ):
     r, c = lax.axis_index("ra"), lax.axis_index("cb")
@@ -151,12 +151,6 @@
     exchange_tall(0)
     all_of(tokens4_v.at[pl.ds(0, NY - 1)], recv_sem.at[4])
     stream0 = tokens4_v[...].reshape(NY * FEATURES, TOKENS).astype(F32)
-    own_square = over_features(stream0 * stream0)
-    square_v[...] = own_square
-    for dz in Z_ORDER:
-        push(square_v, squares_v.at[z], 6, to_z(dz)[1])
-    squares_v[z] = own_square
-    pending.append((squares_v.at[pl.ds(0, NZ - 1)], send_sem.at[6]))
     arrange_wide(1)
     exchange_wide(1)
     arrange_tall(1)
@@ -177,14 +171,12 @@
         lax.broadcasted_iota(jnp.int32, (128, 128), 0) == lax.broadcasted_iota(jnp.int32, (128, 128), 1) - STAT, 1.0, 0.0
     ).astype(BF16)
 
-    def multiply(l, slot, features, statistics, exact):
+    def multiply(l, slot, features, statistics):
         left = features.T
         high = left.astype(BF16)
         wide = wide_v[l].reshape(NY * FEATURES, 384)
-        part = jnp.dot(high, wide, preferred_element_type=F32)
-        if not exact:
-            low = (left - high.astype(F32)).astype(BF16)
-            part = part + jnp.dot(low, wide, preferred_element_type=F32)
+        low = (left - high.astype(F32)).astype(BF16)
+        part = jnp.dot(high, wide, preferred_element_type=F32) + jnp.dot(low, wide, preferred_element_type=F32)
         last = part[:, 256:384]
         if statistics:
             lines = [t for s in statistics for t in terms(s)]
@@ -254,32 +246,55 @@
             acc = acc + parts_v[l, k].astype(F32)
         return acc
 
+    xy = [(dy, dx, dk) for dy in (2, 1, 3, 0) for dx in (2, 1, 3, 0) for dk in (0, 1) if dy or dx or dk]
+
+    def to_xy(step):
+        dy, dx, dk = step
+        there_y = lax.rem(y + dy, NY)
+        there_c = lax.rem(c // 2 + dx, 4) * 2 + lax.rem(c % 2 + dk, 2)
+        return there_y, there_c, {"ra": z * NY + there_y, "cb": there_c}
+
+    def scatter_xy(part):
+        shared_v[...] = part.reshape(NY, NC, 8, TOKENS)
+        for k, step in enumerate(xy):
+            there_y, there_c, device = to_xy(step)
+            push(shared_v.at[there_y, there_c], shares_v.at[k], 12, device)
+        pending.append((shares_v, send_sem.at[12]))
+
+    def total_xy():
+        all_of(shares_v, recv_sem.at[12])
+        acc = shared_v[y, c]
+        for k in range(len(xy)):
+            acc = acc + shares_v[k]
+        return acc
+
+    def gather_xy(block):
+        block_v[...] = block
+        for step in xy:
+            push(block_v, branch_v.at[y, c], 16, to_xy(step)[2])
+        branch_v[y, c] = block
+        pending.append((shares_v, send_sem.at[16]))
+        all_of(shares_v, recv_sem.at[16])
+
     gains = [gain(i) for i in range(3)]
-    all_of(squares_v.at[pl.ds(0, NZ - 1)], recv_sem.at[6])
-    squares = squares_v[0]
-    for k in range(1, NZ):
-        squares = squares + squares_v[k]
-    scale = lax.rsqrt(squares / D + EPSILON)
     all_of(wide_v.at[0, pl.ds(0, NY - 1)], recv_sem.at[0])
-    multiply(0, 0, stream0 * scale * gains[0], [], True)
+    multiply(0, 0, stream0 * gains[0], [over_features(stream0 * stream0)])
     scatter(0)
+    acc = total(0)
+    squares = joined(acc[:, 256:384], STAT)
+    acc = acc * lax.rsqrt(squares / D + EPSILON)
+    broadcast_hidden(0, acc, None)
     all_of(wide_v.at[1, pl.ds(0, NY - 1)], recv_sem.at[1])
-    multiply(1, 1, stream0 * gains[1], [own_square], False)
-    acc = total(0)
-    broadcast_hidden(0, acc, None)
+    multiply(1, 1, stream0 * gains[1], [])
     scatter(1)
     part = project(0)
-    block = branch_total(0, part)
-    block_v[...] = block
-    for dy in Y_ORDER:
-        push(block_v, branch_v.at[y], 16, to_y(dy)[1])
-    branch_v[y] = block
-    pending.append((branch_v.at[pl.ds(0, NY - 1)], send_sem.at[16]))
-    all_of(branch_v.at[pl.ds(0, NY - 1)], recv_sem.at[16])
+    scatter_xy(part)
+    block = total_xy()
+    gather_xy(block)
     branch = branch_v[...].reshape(NY * FEATURES, TOKENS)
     gained = branch * gains[2]
 
-    multiply(1, 2, gained * gains[1], [over_features(branch * branch), over_features(gained * gained), over_features(stream0 * gained)], False)
+    multiply(1, 2, gained * gains[1], [over_features(branch * branch), over_features(gained * gained), over_features(stream0 * gained)])
     scatter(2)
     stream_v[...] = stream0.reshape(NY, FEATURES, TOKENS)
     gained_v[...] = gained.reshape(NY, FEATURES, TOKENS)
@@ -288,7 +303,7 @@
     rest = acc[:, 256:384]
     scale_out = lax.rsqrt(joined(rest, STAT) / D + EPSILON)
     squares = (
-        RESIDUAL * RESIDUAL * joined(early[:, 256:384], STAT)
+        RESIDUAL * RESIDUAL * squares
         + 2.0 * RESIDUAL * scale_out * joined(rest, STAT + 6)
         + scale_out * scale_out * joined(rest, STAT + 3)
     )
@@ -347,8 +362,6 @@
             pltpu.VMEM((2, NY, FEATURES, 384), BF16),
             pltpu.VMEM((2, NY, FEATURES, 256), BF16),
             pltpu.VMEM((2, NY, FEATURES, 256), BF16),
-            pltpu.VMEM((1, TOKENS), F32),
-            pltpu.VMEM((NZ, 1, TOKENS), F32),
             pltpu.VMEM((3, NZ, ROWS, 384), BF16),
             pltpu.VMEM((3, NZ, ROWS, 384), BF16),
             pltpu.VMEM((2, ROWS, 256), BF16),
@@ -358,8 +371,10 @@
             pltpu.VMEM((2, NY, FEATURES, TOKENS), BF16),
             pltpu.VMEM((2, FEATURES, TOKENS), BF16),
             pltpu.VMEM((2, NC, FEATURES, TOKENS), BF16),
-            pltpu.VMEM((FEATURES, TOKENS), F32),
-            pltpu.VMEM((NY, FEATURES, TOKENS), F32),
+            pltpu.VMEM((8, TOKENS), F32),
+            pltpu.VMEM((NY, NC, 8, TOKENS), F32),
+            pltpu.VMEM((NY, NC, 8, TOKENS), F32),
+            pltpu.VMEM((NR - 1, 8, TOKENS), F32),
             pltpu.VMEM((NY, FEATURES, TOKENS), F32),
             pltpu.VMEM((NY, FEATURES, TOKENS), F32),
             pltpu.VMEM((1, TOKENS), F32),

time: 66.8 us -> 61.9 us (0.927)
  Pallas kernels: 65.3 us -> 60.4 us
    pallas_call x1, Pallas kernels: 65.3 us -> 60.4 us  [per_device(): pl.pallas_call(kernel, out_shape=jax.ShapeDtypeStruct((FEATURES, TOKENS),...]
where the time goes in v3:
time: 61.9 us; the launch traced here: 61.7 us
  Pallas kernels  60.4 us (98%)
  local copies, waits for them, and re-layouts  1.32 us (2%)
    pallas_call x1, Pallas kernels, per_device(): pl.pallas_call(kernel, out_shape=jax.ShapeDtypeStruct((FEATURES, TOKENS),...  60.4 us
    unnamed x1, local copies, waits for them, and re-layouts  1.32 us

profile of v3, /device:TPU:1, one launch (start us, length us, event | category | flops | bytes accessed | tf_op | source)
XLA Modules:
  0.0 61.7 jit_solution(7919835271589030334)
XLA Ops:
  0.0 60.4 %shard_map.64 = bf16[64,128]{1,0:T(8,128)(2,1)} custom-call(bf16[64,128]{1,0:T(8,128)(2,1)} %bitcast.5, f32[2,64]{1,0:T(2,128)} %pre_hbm.1, f32[2,64]{1,0:T(2,128)} %post_hbm.1, bf16[2,64,704]{2,1,0:T(8,128)(2,1)} %gate_hbm.1, bf16[2,64,704]{2,1,0:T(8,128)(2,1)} %up_hbm.1, bf16[2,64,704]{2,1,0:T(8,128)(2,1)} %bitcast.3), custom_call_target="tpu_custom_call" | custom-call | tf_op jit(solution)/shard_map/pallas_call | solution.py:348
  60.4 1.3 %copy.8 = bf16[128,64]{0,1:T(8,128)(2,1)} copy(bf16[128,64]{0,1:T(8,128)(2,1)} %bitcast.4) | data formatting | bytes 32768

commit v4 on v3

--- a/solution.py
+++ b/solution.py
@@ -52,7 +52,7 @@
     wide_from_v, wide_v, tall_from_v, tall_v,
     sent_v, got_v, mine_v, hidden_v,
     piece_v, own_v, pieces_v, part_v, parts_v, block_v, branch_v, shared_v, shares_v, stream_v, gained_v, norm_v, norms_v,
-    load_sem, send_sem, recv_sem,
+    load_sem, send_sem, recv_sem, near_sem, far_sem,
 ):
     r, c = lax.axis_index("ra"), lax.axis_index("cb")
     z, y = r // NY, r % NY
@@ -77,7 +77,7 @@
         ).start()
 
     barrier = pltpu.get_barrier_semaphore()
-    for device in [to_z(k)[1] for k in range(1, NZ)] + [to_y(k)[1] for k in range(1, NY)] + [to_c(k)[1] for k in range(1, NC)]:
+    for device in [to_z(k)[1] for k in (1, NZ - 1)] + [to_y(k)[1] for k in range(1, NY)] + [to_c(k)[1] for k in range(1, NC)]:
         pl.semaphore_signal(barrier, inc=1, device_id=device, device_id_type=MESH)
 
     loads = [
@@ -135,7 +135,7 @@
     arrange_wide(0)
     for load in loads[2:]:
         load.wait()
-    pl.semaphore_wait(barrier, NZ - 1 + NY - 1 + NC - 1)
+    pl.semaphore_wait(barrier, 2 + NY - 1 + NC - 1)
 
 
     for dy in Y_ORDER:
@@ -146,15 +146,16 @@
     pending.append((tokens4_v.at[pl.ds(0, NY - 1)], send_sem.at[4]))
     pending.append((gains4_v.at[pl.ds(0, NY - 1)], send_sem.at[5]))
     exchange_wide(0)
-
+    for dz in (1, NZ - 1):
+        pl.semaphore_signal(near_sem, inc=1, device_id=to_z(dz)[1], device_id_type=MESH)
     arrange_tall(0)
-    exchange_tall(0)
+    pl.semaphore_wait(near_sem, 2)
+    for dz in (2, NZ - 2):
+        pl.semaphore_signal(far_sem, inc=1, device_id=to_z(dz)[1], device_id_type=MESH)
+    arrange_wide(1)
+    arrange_tall(1)
     all_of(tokens4_v.at[pl.ds(0, NY - 1)], recv_sem.at[4])
     stream0 = tokens4_v[...].reshape(NY * FEATURES, TOKENS).astype(F32)
-    arrange_wide(1)
-    exchange_wide(1)
-    arrange_tall(1)
-    exchange_tall(1)
 
     all_of(gains4_v.at[pl.ds(0, NY - 1)], recv_sem.at[5])
     lines = []
@@ -165,7 +166,6 @@
 
     def gain(i):
         return jnp.concatenate([columns[:, 8 * q + i : 8 * q + i + 1] for q in range(NY)], axis=0)
-
 
     passing = jnp.where(
         lax.broadcasted_iota(jnp.int32, (128, 128), 0) == lax.broadcasted_iota(jnp.int32, (128, 128), 1) - STAT, 1.0, 0.0
@@ -279,7 +279,11 @@
     gains = [gain(i) for i in range(3)]
     all_of(wide_v.at[0, pl.ds(0, NY - 1)], recv_sem.at[0])
     multiply(0, 0, stream0 * gains[0], [over_features(stream0 * stream0)])
+    pl.semaphore_wait(far_sem, 2)
     scatter(0)
+    exchange_tall(0)
+    exchange_wide(1)
+    exchange_tall(1)
     acc = total(0)
     squares = joined(acc[:, 256:384], STAT)
     acc = acc * lax.rsqrt(squares / D + EPSILON)
@@ -382,6 +386,8 @@
             pltpu.SemaphoreType.DMA((6,)),
             pltpu.SemaphoreType.DMA((18,)),
             pltpu.SemaphoreType.DMA((18,)),
+            pltpu.SemaphoreType.REGULAR,
+            pltpu.SemaphoreType.REGULAR,
         ],
         compiler_params=pltpu.CompilerParams(collective_id=0, has_side_effects=True),
     )(tokens.T, pre_gain, post_gain, gate_weight, up_weight, down_weight.swapaxes(1, 2))

time: 61.9 us -> 60.3 us (0.974)
  Pallas kernels: 60.4 us -> 58.8 us
    pallas_call x1, Pallas kernels: 60.4 us -> 58.8 us  [per_device(): pl.pallas_call(kernel, out_shape=jax.ShapeDtypeStruct((FEATURES, TOKENS),...]
where the time goes in v4:
time: 60.3 us; the launch traced here: 60.1 us
  Pallas kernels  58.8 us (98%)
  local copies, waits for them, and re-layouts  1.32 us (2%)
    pallas_call x1, Pallas kernels, per_device(): pl.pallas_call(kernel, out_shape=jax.ShapeDtypeStruct((FEATURES, TOKENS),...  58.8 us
    unnamed x1, local copies, waits for them, and re-layouts  1.32 us

profile of v4, /device:TPU:1, one launch (start us, length us, event | category | flops | bytes accessed | tf_op | source)
XLA Modules:
  0.0 60.1 jit_solution(7097430726790053639)
XLA Ops:
  0.0 58.8 %shard_map.64 = bf16[64,128]{1,0:T(8,128)(2,1)} custom-call(bf16[64,128]{1,0:T(8,128)(2,1)} %bitcast.5, f32[2,64]{1,0:T(2,128)} %pre_hbm.1, f32[2,64]{1,0:T(2,128)} %post_hbm.1, bf16[2,64,704]{2,1,0:T(8,128)(2,1)} %gate_hbm.1, bf16[2,64,704]{2,1,0:T(8,128)(2,1)} %up_hbm.1, bf16[2,64,704]{2,1,0:T(8,128)(2,1)} %bitcast.3), custom_call_target="tpu_custom_call" | custom-call | tf_op jit(solution)/shard_map/pallas_call | solution.py:352
  58.8 1.3 %copy.8 = bf16[128,64]{0,1:T(8,128)(2,1)} copy(bf16[128,64]{0,1:T(8,128)(2,1)} %bitcast.4) | data formatting | bytes 32768
